TPU v7x, 32 devices: a whole 2x2x4 slice. The times are simulated.
32 devices in a mesh: rep: 16 (over z, y, core), fs: 2 (over x), tp: 1.
Axes of the slice: x: 2, y: 2, z: 4, core: 2. Of those that a mesh axis runs over, the one named last changes fastest.
Arguments:
- pre_act: bfloat16 [16384, 4096], P('rep', ('fs', 'tp')), may hold values from -6 to 6
- down_weight: bfloat16 [4096, 2048], P(('fs', 'tp')), may hold values from -0.09375 to 0.09375
- cotangent: bfloat16 [16384, 2048], P('rep', ('fs', 'tp')), may hold values from -6 to 6
Outputs:
- grad_pre: bfloat16 [16384, 4096], P('rep', ('fs', 'tp'))
- grad_weight: float32 [4096, 2048], P(('fs', 'tp', 'rep'))
All inputs are finite; a program needn't handle non-finite values.
Results may differ from a plain program's by a relative error of at most 0.0029.
Values may be sent and summed in bfloat16 or wider, within the bound.
A program may use at most 128 MiB of HBM per device.

v0:
```python
import jax
import jax.numpy as jnp
from jax import lax
from jax.sharding import PartitionSpec as P


def on_device(pre_act, down_weight, cotangent):
    whole = lax.all_gather(cotangent, ("fs", "tp"), axis=1, tiled=True)
    grad_hidden = lax.dot_general(
        whole, down_weight, (((1,), (1,)), ((), ())), preferred_element_type=jnp.float32
    )
    positive = jnp.maximum(pre_act.astype(jnp.float32), 0.0)
    grad_pre = (grad_hidden * 2.0 * positive).astype(jnp.bfloat16)
    hidden = (positive * positive).astype(jnp.bfloat16)
    factor = 1.0 / jnp.sqrt(jnp.float32(pre_act.shape[0] * lax.axis_size("rep")))
    term = lax.dot_general(
        hidden, whole, (((0,), (0,)), ((), ())), preferred_element_type=jnp.float32
    )
    summed = lax.psum_scatter(term, "rep", scatter_dimension=0, tiled=True)
    return (grad_pre, summed * factor)


def solution(mesh):
    return jax.shard_map(
        on_device,
        mesh=mesh,
        in_specs=(P("rep", ("fs", "tp")), P(("fs", "tp"), None), P("rep", ("fs", "tp"))),
        out_specs=(P("rep", ("fs", "tp")), P(("fs", "tp", "rep"), None)),
        check_vma=False,
    )
```

profile of v0, /device:TPU:0, one launch (start us, length us, event | category | flops | bytes accessed | tf_op | source)
XLA Modules:
  0.0 270.9 jit_solution(17533116220339422526)
XLA Ops:
  7.2 0.0 all-gather.2.cloned.1.call-start
  7.2 0.7 all-gather.2.cloned.1.call-update
  7.9 0.0 reduce-scatter.2.cloned.1.call-start
  7.9 61.0 %all-gather.2.cloned.1.call-done = bf16[1024,2048]{1,0:T(8,128)(2,1)} async-done(((bf16[1024,1024]{1,0:T(8,128)(2,1)}), bf16[1024,2048]{1,0:T(8,128)(2,1)}) %all-gather.2.cloned.1.call-update) | async-done | bytes 4194320 | tf_op jit(solution)/shard_map/all_gather | solution.py:8
  69.0 15.2 %fusion = f32[2048,2048]{1,0:T(8,128)} fusion(bf16[1024,2048]{1,0:T(8,128)(2,1)} %all-gather.2.cloned.1.call-done, bf16[1024,2048]{1,0:T(8,128)(2,1)} %param.3), kind=kOutput, calls=%fused_computation.3 | convolution fusion | flops 8598323200 | bytes 25165824 | tf_op jit(solution)/shard_map/dot_general | solution.py:16
  84.2 0.0 reduce-scatter.2.cloned.1.call-update
  84.2 14.5 %multiply_convert_fusion.1 = bf16[1024,2048]{1,0:T(8,128)(2,1)} fusion(bf16[1024,2048]{1,0:T(8,128)(2,1)} %param.3, bf16[1024,2048]{1,0:T(8,128)(2,1)} %all-gather.2.cloned.1.call-done, bf16[2048,2048]{1,0:T(8,128)(2,1)} %param.4), kind=kOutput, calls=%fused_computation.1 | convolution fusion | flops 8600420352 | bytes 20971520 | tf_op jit(solution)/shard_map/dot_general | solution.py:9
  98.8 163.0 %reduce-scatter.2.cloned.1.call-done = f32[128,2048]{1,0:T(8,128)} async-done(((f32[2048,2048]{1,0:T(8,128)}), f32[128,2048]{1,0:T(8,128)}) %reduce-scatter.2.cloned.1.call-update) | async-done | bytes 1048592 | tf_op jit(solution)/shard_map/reduce_scatter | solution.py:19
  261.7 2.3 broadcast_multiply_fusion
Async XLA Ops:
  7.2 61.8 %all-gather.2.cloned.1.call-start = ((), (), s32[]{:S(2)}) async-start(), calls=%async_computation.1 | async-start | bytes 6291456 | tf_op jit(solution)/shard_map/all_gather | solution.py:8
  7.9 253.8 %reduce-scatter.2.cloned.1.call-start = ((), (), s32[]{:S(2)}) async-start(), calls=%async_computation.2 | async-start | bytes 17825792 | tf_op jit(solution)/shard_map/reduce_scatter | solution.py:19
Sparse Core Ops, SparseCore 0:
  9.5 59.4 all-gather.1
  84.3 177.3 reduce-scatter.1
where the time goes:
time: 271 us
  waiting for transfers between devices  225 us (83%)
  matrix products  29.7 us (11%)
  between operations  14 us (5%)
    reduce_scatter x1, waiting for transfers between devices, on_device(): summed = lax.psum_scatter(term, 'rep', scatter_dimension=0, tiled=True)  163 us
    all_gather x1, waiting for transfers between devices, on_device(): whole = lax.all_gather(cotangent, ('fs', 'tp'), axis=1, tiled=True)  61 us
    dot_general x1, matrix products, on_device(): lax.dot_general(hidden, whole, (((0,), (0,)), ((), ())), preferred_elemen...  15.2 us
    dot_general x1, matrix products, on_device(): lax.dot_general(whole, down_weight, (((1,), (1,)), ((), ())), preferred_e...  14.5 us
  transfers between devices with their start and end apart: 2, of which 2 were waited for; matrix products, arithmetic and copies ran while one was open for 5% of the time, Pallas kernels for 0%

commit v1 on v0

v1 whole, which is shorter than its diff:
```python
import functools

import jax
import jax.numpy as jnp
from jax import lax
from jax.experimental import pallas as pl
from jax.experimental.pallas import tpu as pltpu
from jax.sharding import PartitionSpec as P

MESH = pl.DeviceIdType.MESH
CORES, ROWS = 2, 2
F32, BF16 = jnp.float32, jnp.bfloat16


def chunks_of(width, sizes):
    out, at = [], 0
    for s in sizes:
        out.append((at, s))
        at += s
    assert at == width
    return out


def plain(pre_act, down_weight, cotangent):
    whole = lax.all_gather(cotangent, ("fs", "tp"), axis=1, tiled=True)
    grad_hidden = lax.dot_general(
        whole, down_weight, (((1,), (1,)), ((), ())), preferred_element_type=F32
    )
    positive = jnp.maximum(pre_act.astype(F32), 0.0)
    grad_pre = (grad_hidden * 2.0 * positive).astype(BF16)
    hidden = (positive * positive).astype(BF16)
    factor = 1.0 / jnp.sqrt(jnp.float32(pre_act.shape[0] * lax.axis_size("rep")))
    term = lax.dot_general(
        hidden, whole, (((0,), (0,)), ((), ())), preferred_element_type=F32
    )
    summed = lax.psum_scatter(term, "rep", scatter_dimension=0, tiled=True)
    return (grad_pre, summed * factor)


def kernel(
    depth, near, far, factor,
    pre_hbm, w_hbm, cot_hbm, gp_hbm, gw_hbm,
    pre, pre_in, turned, w, cot, grad, gp,
    y_out, y_in, own, z_out, z_in, gw,
    s_local, s_pre_s, s_pre_r, s_near_s, s_near_r, s_x_s, s_x_r, s_fwd_s, s_fwd_r,
    s_y_s, s_y_r, s_z_s, s_z_r, s_gp,
):
    rep, fs, tp = lax.axis_index("rep"), lax.axis_index("fs"), lax.axis_index("tp")
    c, y, z = rep % CORES, (rep // CORES) % ROWS, rep // (CORES * ROWS)
    tokens, half = cot_hbm.shape
    hid = w_hbm.shape[0]
    block = own.shape[1]
    blocks = 2 * depth

    def at(z_, y_, c_, f_):
        return ((z_ * ROWS + y_) * CORES + c_, f_, tp)

    partner, across, beside = at(z, y, 1 - c, fs), at(z, y, c, 1 - fs), at(z, 1 - y, c, fs)

    def remote(src, dst, s, r, to):
        return pltpu.make_async_remote_copy(
            src_ref=src, dst_ref=dst, send_sem=s, recv_sem=r, device_id=to, device_id_type=MESH
        )

    def columns(i, c_):
        y_ = (1 - y) if i < depth else y
        k = (i % depth) * ROWS + y_
        return pl.ds(pl.multiple_of((k * CORES + c_) * block, block), block)

    def local(i, src, dst):
        return pltpu.make_async_copy(src, dst, s_local.at[i])

    loads = [local(0, pre_hbm, pre), local(1, cot_hbm, cot.at[0, pl.ds(0, tokens)]), local(2, w_hbm, w)]
    for l in loads:
        l.start()

    barrier = pltpu.get_barrier_semaphore()
    peers = [partner, across, beside]
    for d in range(1, depth):
        peers.append(at((z + d) % depth, y, c, fs))
    for p in peers:
        pl.semaphore_signal(barrier, inc=1, device_id=p, device_id_type=MESH)
    pl.semaphore_wait(barrier, len(peers))

    x_copies = []
    for q, (a, n) in enumerate(far):
        x_copies.append(remote(
            cot_hbm.at[:, pl.ds(a, n)], cot.at[1, pl.ds(0, tokens), pl.ds(a, n)],
            s_x_s.at[q], s_x_r.at[q], across))
    x_copies[0].start()
    pre_copies = []
    for i in range(blocks):
        pre_copies.append(remote(
            pre_hbm.at[:, columns(i, 1 - c)], pre_in.at[i], s_pre_s.at[i], s_pre_r.at[i], partner))
        pre_copies[-1].start()
    near_copies = []
    for q, (a, n) in enumerate(near):
        near_copies.append(remote(
            cot_hbm.at[:, pl.ds(a, n)], cot.at[0, pl.ds(tokens, tokens), pl.ds(a, n)],
            s_near_s.at[q], s_near_r.at[q], partner))
        near_copies[-1].start()
    for xc in x_copies[1:]:
        xc.start()

    def turn(v):
        p = jnp.maximum(v.astype(F32), 0.0)
        return (p * p).T.astype(BF16)

    strip = 256

    loads[0].wait()
    for i in range(blocks):
        cols = columns(i, c)

        @pl.loop(0, tokens // strip)
        def _(t):
            rows = pl.ds(pl.multiple_of(t * strip, strip), strip)
            turned[pl.ds(i * block, block), rows] = turn(pre[rows, cols])

    loads[1].wait()
    loads[2].wait()
    for pc in pre_copies:
        pc.wait_recv()

    @pl.loop(0, blocks)
    def _(i):
        @pl.loop(0, tokens // strip)
        def _(t):
            rows = pl.ds(pl.multiple_of(t * strip, strip), strip)
            to = pl.ds(pl.multiple_of(tokens + t * strip, strip), strip)
            turned[pl.ds(pl.multiple_of(i * block, block), block), to] = turn(pre_in[i, rows, :])

    tall = 2 * block

    chunks = [(0, a, n) for a, n in near] + [(1, a, n) for a, n in far]

    def span(h, a, n):
        return pl.ds(h * half + a, n)

    def y_copy(j):
        h, a, n = chunks[j]
        s = span(h, a, n)
        return remote(y_out.at[:, :, s], y_in.at[:, :, s], s_y_s.at[j], s_y_r.at[j], beside)

    def z_copy(j, d):
        h, a, n = chunks[j]
        s = span(h, a, n)
        to = (z + d) % depth
        return remote(
            z_out.at[to, :, s], z_in.at[d - 1, :, s],
            s_z_s.at[j * (depth - 1) + d - 1], s_z_r.at[j * (depth - 1) + d - 1], at(to, y, c, fs))

    def fwd_copy(q):
        a, n = far[q]
        return remote(
            cot.at[1, pl.ds(0, tokens), pl.ds(a, n)], cot.at[1, pl.ds(tokens, tokens), pl.ds(a, n)],
            s_fwd_s.at[q], s_fwd_r.at[q], partner)

    def product(j):
        h, a, n = chunks[j]
        s = span(h, a, n)

        def dot(m):
            rows = pl.ds(pl.multiple_of(m * tall, tall), tall)
            return lax.dot_general(
                turned[rows, :], cot[h, :, pl.ds(a, n)], (((1,), (0,)), ((), ())),
                preferred_element_type=F32).reshape(2, block, n)

        @pl.loop(0, depth // 2)
        def _(m):
            y_out[pl.ds(m * 2, 2), :, s] = dot(m).astype(BF16)

        y_copy(j).start()

        @pl.loop(0, depth // 2)
        def _(m):
            own[pl.ds(m * 2, 2), :, s] = dot(m + depth // 2)

    def second(j):
        h, a, n = chunks[j]
        s = span(h, a, n)
        y_copy(j).wait_recv()

        @pl.loop(0, depth)
        def _(k):
            v = own[k, :, s] + y_in[k, :, s].astype(F32)
            own[k, :, s] = v
            z_out[k, :, s] = v.astype(BF16)

        for d in range(1, depth):
            z_copy(j, d).start()

    def last(j):
        h, a, n = chunks[j]
        s = span(h, a, n)
        for d in range(1, depth):
            z_copy(j, d).wait_recv()
        v = own[z, :, s]
        for d in range(depth - 1):
            v = v + z_in[d, :, s].astype(F32)
        place = pl.multiple_of((fs if h == 0 else 1 - fs) * half + a, 128)
        gw[:, pl.ds(place, n)] = v * factor

    tm, tn = 256, 512

    def grad_tile(h, a, n, m, k):
        rows = pl.ds(pl.multiple_of(m * tm, tm), tm)
        outs = pl.ds(pl.multiple_of(k * tn, tn), tn)
        place = pl.multiple_of((fs if h == 0 else 1 - fs) * half + a, 128)
        return rows, outs, lax.dot_general(
            cot[h, rows, pl.ds(a, n)], w[outs, pl.ds(place, n)], (((1,), (1,)), ((), ())),
            preferred_element_type=F32)

    def grad_first():
        @pl.loop(0, tokens // tm)
        def _(m):
            @pl.loop(0, hid // tn)
            def _(k):
                rows, outs, v = grad_tile(0, 0, half, m, k)
                grad[rows, outs] = v

    def gp_copy(m):
        rows = pl.ds(pl.multiple_of(m * tm, tm), tm)
        return pltpu.make_async_copy(gp.at[rows], gp_hbm.at[rows], s_gp.at[m])

    def grad_rest():
        @pl.loop(0, tokens // tm)
        def _(m):
            @pl.loop(0, hid // tn)
            def _(k):
                rows, outs, v = grad_tile(1, 0, half, m, k)
                p = jnp.maximum(pre[rows, outs].astype(F32), 0.0)
                gp[rows, outs] = ((grad[rows, outs] + v) * 2.0 * p).astype(BF16)
            gp_copy(m).start()

    nn, nf = len(near), len(far)
    for q in range(nn):
        near_copies[q].wait_recv()
        product(q)
    grad_first()

    done2 = 0
    done3 = 0
    for q in range(nf):
        while done2 < min(nn + q - 1, (q * (nn + nf)) // nf):
            second(done2)
            done2 += 1
        x_copies[q].wait_recv()
        fwd_copy(q).start()
        fwd_copy(q).wait_recv()
        product(nn + q)
    grad_rest()
    total = nn + nf
    while done2 < total:
        second(done2)
        done2 += 1
        while done3 < done2 - 2:
            last(done3)
            done3 += 1
    while done3 < total:
        last(done3)
        done3 += 1
    out = local(3, gw, gw_hbm)
    out.start()

    for copy in pre_copies + near_copies + x_copies:
        copy.wait_send()
    for q in range(nf):
        fwd_copy(q).wait_send()
    for j in range(total):
        y_copy(j).wait_send()
        for d in range(1, depth):
            z_copy(j, d).wait_send()

    @pl.loop(0, tokens // tm)
    def _(m):
        gp_copy(m).wait()
    out.wait()


def solution(mesh):
    reps, fs, tp = mesh.shape["rep"], mesh.shape["fs"], mesh.shape["tp"]
    depth = reps // (CORES * ROWS)

    def on_device(pre_act, down_weight, cotangent):
        tokens, hid = pre_act.shape
        half = cotangent.shape[1]
        width = down_weight.shape[1]
        block = hid // reps
        if not (fs == 2 and tp == 1 and depth * CORES * ROWS == reps and depth % 2 == 0
                and block % 128 == 0 and half % 1024 == 0 and hid % 512 == 0 and tokens % 256 == 0):
            return plain(pre_act, down_weight, cotangent)
        step = half // 4
        near = chunks_of(half, [step] * 4)
        far = chunks_of(half, [step] * 3 + [step // 2] * 2)
        nn, nf = len(near), len(far)
        total = nn + nf
        factor = 1.0 / float(tokens * reps) ** 0.5
        dma = lambda n: pltpu.SemaphoreType.DMA((n,))
        vm = pltpu.VMEM
        return pl.pallas_call(
            functools.partial(kernel, depth, near, far, factor),
            out_shape=[
                jax.ShapeDtypeStruct((tokens, hid), BF16),
                jax.ShapeDtypeStruct((block, width), F32),
            ],
            in_specs=[pl.BlockSpec(memory_space=pl.ANY)] * 3,
            out_specs=[pl.BlockSpec(memory_space=pl.ANY)] * 2,
            scratch_shapes=[
                vm((tokens, hid), BF16),
                vm((2 * depth, tokens, block), BF16),
                vm((2 * depth * block, 2 * tokens), BF16),
                vm(down_weight.shape, BF16),
                vm((2, 2 * tokens, half), BF16),
                vm((tokens, hid), F32),
                vm((tokens, hid), BF16),
                vm((depth, block, width), BF16),
                vm((depth, block, width), BF16),
                vm((depth, block, width), F32),
                vm((depth, block, width), BF16),
                vm((depth - 1, block, width), BF16),
                vm((block, width), F32),
                dma(4), dma(2 * depth), dma(2 * depth), dma(nn), dma(nn), dma(nf), dma(nf), dma(nf), dma(nf),
                dma(total), dma(total), dma(total * (depth - 1)), dma(total * (depth - 1)),
                dma(tokens // 256),
            ],
            compiler_params=pltpu.CompilerParams(
                collective_id=0, has_side_effects=True, vmem_limit_bytes=66 * 1000 * 1000
            ),
            cost_estimate=pl.CostEstimate(
                flops=8 * tokens * hid * width // 2, bytes_accessed=40 * 1024 * 1024, transcendentals=0),
        )(pre_act, down_weight, cotangent)

    return jax.shard_map(
        on_device,
        mesh=mesh,
        in_specs=(P("rep", ("fs", "tp")), P(("fs", "tp"), None), P("rep", ("fs", "tp"))),
        out_specs=(P("rep", ("fs", "tp")), P(("fs", "tp", "rep"), None)),
        check_vma=False,
    )
```

time: 271 us -> 86 us (0.32)
  waiting for transfers between devices: 225 us -> 0 us
  Pallas kernels: 0 us -> 79.4 us
  matrix products: 29.7 us -> 0 us
  between operations: 14 us -> 0.65 us
  local copies, waits for them, and re-layouts: 0 us -> 5.85 us
    reduce_scatter x1 -> x0, waiting for transfers between devices: 163 us -> none  [on_device(): summed = lax.psum_scatter(term, 'rep', scatter_dimension=0, tiled=True)]
    pallas_call x0 -> x1, Pallas kernels: none -> 79.4 us  [on_device(): pl.pallas_call(functools.partial(kernel, depth, near, far, factor), out_s...]
    all_gather x1 -> x0, waiting for transfers between devices: 61 us -> none  [on_device(): whole = lax.all_gather(cotangent, ('fs', 'tp'), axis=1, tiled=True)]
    dot_general x2 -> x0, matrix products: 29.7 us -> none  [the longest x1 15.2 us: on_device(): lax.dot_general(hidden, whole, (((0,), (0,)), ((), ())), preferred_elemen...]
    unnamed x0 -> x4, local copies, waits for them, and re-layouts: none -> 5.85 us
  transfers between devices with their start and end apart: 2 -> 0, of which waited for: 2 -> 0; matrix products, arithmetic and copies ran while one was open for 5% -> 0% of each run, Pallas kernels for 0% -> 0%
where the time goes in v1:
time: 86 us; the launch traced here: 85.9 us
  Pallas kernels  79.4 us (92%)
  local copies, waits for them, and re-layouts  5.85 us (7%)
    pallas_call x1, Pallas kernels, on_device(): pl.pallas_call(functools.partial(kernel, depth, near, far, factor), out_s...  79.4 us
    unnamed x4, local copies, waits for them, and re-layouts  5.85 us

profile of v1, /device:TPU:0, one launch (start us, length us, event | category | flops | bytes accessed | tf_op | source)
XLA Modules:
  0.0 85.9 jit_solution(17928515393179753674)
XLA Ops:
  0.6 79.4 %shard_map.50 = (bf16[1024,2048]{1,0:T(8,128)(2,1)}, f32[128,2048]{1,0:T(8,128)}) custom-call(bf16[1024,2048]{1,0:T(8,128)(2,1)} %pre_hbm.1, bf16[2048,2048]{1,0:T(8,128)(2,1)} %w_hbm.1, bf16[1024,1024]{1,0:T(8,128)(2,1)} %cot_hbm.1), custom_call_target="tpu_custom_call" | custom-call | flops 17179869184 | bytes 41943040 | tf_op jit(solution)/shard_map/pallas_call | solution.py:301
  80.0 0.0 copy-start
  80.0 4.9 %copy.7 = bf16[1024,2048]{1,0:T(8,128)(2,1)} copy(bf16[1024,2048]{1,0:T(8,128)(2,1)} %get-tuple-element.4) | data formatting | bytes 8388608
  84.9 0.0 copy-done
  84.9 1.0 %copy.8 = f32[128,2048]{1,0:T(8,128)} copy(f32[128,2048]{1,0:T(8,128)S(1)} %copy-done) | data formatting | bytes 2097152
Async XLA Ops:
  80.0 4.9 %copy-start = (f32[128,2048]{1,0:T(8,128)S(1)}, f32[128,2048]{1,0:T(8,128)}, u32[]{:S(2)}) copy-start(f32[128,2048]{1,0:T(8,128)} %get-tuple-element.5) | copy-start | bytes 3145732

commit v2 on v1

--- a/solution.py
+++ b/solution.py
@@ -10,6 +10,28 @@
 MESH = pl.DeviceIdType.MESH
 CORES, ROWS = 2, 2
 F32, BF16 = jnp.float32, jnp.bfloat16
+
+
+ORDER = (
+    "n0 A0 n1 A1",
+    "o4 i4 B0 B1",
+    "n2 A2 n3 A3",
+    "s0 B2 x0 B3",
+    "f0 A4 B4 s1",
+    "g0 g1 x1 t0",
+    "g2 f1 s2 A5",
+    "B5 t1 g3 h0",
+    "t2 h1 s3 h2",
+    "h3 l0 t3 s4",
+    "x2 l1 f2 A6",
+    "B6 s5 t4 l2",
+    "x3 l3 f3 A7",
+    "B7 s6 x4 t5",
+    "f4 A8 B8 s7",
+    "e0 t6 l4 e1",
+    "s8 e2 l5 l6",
+    "e3 l7 l8",
+)
 
 
 def chunks_of(width, sizes):
@@ -38,7 +60,7 @@
 
 
 def kernel(
-    depth, near, far, factor,
+    depth, near, far, most, order, factor,
     pre_hbm, w_hbm, cot_hbm, gp_hbm, gw_hbm,
     pre, pre_in, turned, w, cot, grad, gp,
     y_out, y_in, own, z_out, z_in, gw,
@@ -108,27 +130,26 @@
 
     strip = 256
 
-    loads[0].wait()
-    for i in range(blocks):
-        cols = columns(i, c)
-
-        @pl.loop(0, tokens // strip)
-        def _(t):
-            rows = pl.ds(pl.multiple_of(t * strip, strip), strip)
-            turned[pl.ds(i * block, block), rows] = turn(pre[rows, cols])
-
-    loads[1].wait()
-    loads[2].wait()
-    for pc in pre_copies:
-        pc.wait_recv()
-
-    @pl.loop(0, blocks)
-    def _(i):
-        @pl.loop(0, tokens // strip)
-        def _(t):
-            rows = pl.ds(pl.multiple_of(t * strip, strip), strip)
-            to = pl.ds(pl.multiple_of(tokens + t * strip, strip), strip)
-            turned[pl.ds(pl.multiple_of(i * block, block), block), to] = turn(pre_in[i, rows, :])
+    def turn_own(first):
+        for i in range(first, first + depth):
+            cols = columns(i, c)
+
+            @pl.loop(0, tokens // strip)
+            def _(t):
+                rows = pl.ds(pl.multiple_of(t * strip, strip), strip)
+                turned[pl.ds(i * block, block), rows] = turn(pre[rows, cols])
+
+    def turn_in(first):
+        for i in range(first, first + depth):
+            pre_copies[i].wait_recv()
+
+        @pl.loop(first, first + depth)
+        def _(i):
+            @pl.loop(0, tokens // strip)
+            def _(t):
+                rows = pl.ds(pl.multiple_of(t * strip, strip), strip)
+                to = pl.ds(pl.multiple_of(tokens + t * strip, strip), strip)
+                turned[pl.ds(pl.multiple_of(i * block, block), block), to] = turn(pre_in[i, rows, :])
 
     tall = 2 * block
 
@@ -142,13 +163,33 @@
         s = span(h, a, n)
         return remote(y_out.at[:, :, s], y_in.at[:, :, s], s_y_s.at[j], s_y_r.at[j], beside)
 
-    def z_copy(j, d):
-        h, a, n = chunks[j]
-        s = span(h, a, n)
-        to = (z + d) % depth
+    slots, far_end = depth, depth - 1
+    inner = (z > 0) & (z < far_end)
+
+    def relayed(j):
+        return j < len(chunks) - 2
+
+    def z_copy(j, kind):
+        h, a, n = chunks[j]
+        s = span(h, a, n)
+        if kind == "up":
+            ends = (z == far_end) if relayed(j) else False
+            block_, slot, to = jnp.where(ends, 0, (z + 1) % depth), jnp.where(ends, 3, 0), jnp.where(ends, far_end - 1, (z + 1) % depth)
+        elif kind == "down":
+            ends = (z == 0) if relayed(j) else False
+            block_, slot, to = jnp.where(ends, far_end, (z + far_end) % depth), jnp.where(ends, 3, 2), jnp.where(ends, 1, (z + far_end) % depth)
+        else:
+            block_, slot, to = (z + 2) % depth, 1, (z + 2) % depth
         return remote(
-            z_out.at[to, :, s], z_in.at[d - 1, :, s],
-            s_z_s.at[j * (depth - 1) + d - 1], s_z_r.at[j * (depth - 1) + d - 1], at(to, y, c, fs))
+            z_out.at[block_, :, s], z_in.at[slot, :, s],
+            s_z_s.at[j * slots + slot], s_z_r.at[j * slots + slot], at(to, y, c, fs))
+
+    def z_arrival(j, slot):
+        h, a, n = chunks[j]
+        s = span(h, a, n)
+        return remote(
+            z_out.at[0, :, s], z_in.at[slot, :, s],
+            s_z_s.at[j * slots + slot], s_z_r.at[j * slots + slot], beside)
 
     def fwd_copy(q):
         a, n = far[q]
@@ -156,7 +197,7 @@
             cot.at[1, pl.ds(0, tokens), pl.ds(a, n)], cot.at[1, pl.ds(tokens, tokens), pl.ds(a, n)],
             s_fwd_s.at[q], s_fwd_r.at[q], partner)
 
-    def product(j):
+    def product(j, mine):
         h, a, n = chunks[j]
         s = span(h, a, n)
 
@@ -166,15 +207,18 @@
                 turned[rows, :], cot[h, :, pl.ds(a, n)], (((1,), (0,)), ((), ())),
                 preferred_element_type=F32).reshape(2, block, n)
 
-        @pl.loop(0, depth // 2)
-        def _(m):
-            y_out[pl.ds(m * 2, 2), :, s] = dot(m).astype(BF16)
-
-        y_copy(j).start()
-
-        @pl.loop(0, depth // 2)
-        def _(m):
-            own[pl.ds(m * 2, 2), :, s] = dot(m + depth // 2)
+        if mine:
+
+            @pl.loop(0, depth // 2)
+            def _(m):
+                own[pl.ds(m * 2, 2), :, s] = dot(m + depth // 2)
+        else:
+
+            @pl.loop(0, depth // 2)
+            def _(m):
+                y_out[pl.ds(m * 2, 2), :, s] = dot(m).astype(BF16)
+
+            y_copy(j).start()
 
     def second(j):
         h, a, n = chunks[j]
@@ -187,19 +231,43 @@
             own[k, :, s] = v
             z_out[k, :, s] = v.astype(BF16)
 
-        for d in range(1, depth):
-            z_copy(j, d).start()
+        z_copy(j, "up").start()
+        z_copy(j, "down").start()
+
+        if relayed(j):
+
+            @pl.when(jnp.logical_not(inner))
+            def _():
+                z_copy(j, "two").start()
+        else:
+            z_copy(j, "two").start()
+
+    def third(j):
+        h, a, n = chunks[j]
+        s = span(h, a, n)
+
+        @pl.when(inner)
+        def _():
+            z_arrival(j, 3).wait_recv()
+            to = (z + 2) % depth
+            z_out[to, :, s] = (own[to, :, s] + z_in[3, :, s].astype(F32)).astype(BF16)
+            z_copy(j, "two").start()
 
     def last(j):
         h, a, n = chunks[j]
         s = span(h, a, n)
-        for d in range(1, depth):
-            z_copy(j, d).wait_recv()
-        v = own[z, :, s]
-        for d in range(depth - 1):
-            v = v + z_in[d, :, s].astype(F32)
+        for slot, there in ((0, z > 0), (2, z < far_end), (1, None)) if relayed(j) else ((0, None), (2, None), (1, None)):
+
+            def add(slot=slot):
+                z_arrival(j, slot).wait_recv()
+                own[z, :, s] = own[z, :, s] + z_in[slot, :, s].astype(F32)
+
+            if there is None:
+                add()
+            else:
+                pl.when(there)(add)
         place = pl.multiple_of((fs if h == 0 else 1 - fs) * half + a, 128)
-        gw[:, pl.ds(place, n)] = v * factor
+        gw[:, pl.ds(place, n)] = own[z, :, s] * factor
 
     tm, tn = 256, 512
 
@@ -211,55 +279,55 @@
             cot[h, rows, pl.ds(a, n)], w[outs, pl.ds(place, n)], (((1,), (1,)), ((), ())),
             preferred_element_type=F32)
 
-    def grad_first():
-        @pl.loop(0, tokens // tm)
-        def _(m):
-            @pl.loop(0, hid // tn)
-            def _(k):
-                rows, outs, v = grad_tile(0, 0, half, m, k)
-                grad[rows, outs] = v
+    def grad_first(m):
+        @pl.loop(0, hid // tn)
+        def _(k):
+            rows, outs, v = grad_tile(0, 0, half, m, k)
+            grad[rows, outs] = v
+
+    def grad_next(m):
+        @pl.loop(0, hid // tn)
+        def _(k):
+            rows, outs, v = grad_tile(1, 0, most, m, k)
+            grad[rows, outs] += v
 
     def gp_copy(m):
-        rows = pl.ds(pl.multiple_of(m * tm, tm), tm)
+        rows = pl.ds(m * tm, tm)
         return pltpu.make_async_copy(gp.at[rows], gp_hbm.at[rows], s_gp.at[m])
 
-    def grad_rest():
-        @pl.loop(0, tokens // tm)
-        def _(m):
-            @pl.loop(0, hid // tn)
-            def _(k):
-                rows, outs, v = grad_tile(1, 0, half, m, k)
-                p = jnp.maximum(pre[rows, outs].astype(F32), 0.0)
-                gp[rows, outs] = ((grad[rows, outs] + v) * 2.0 * p).astype(BF16)
-            gp_copy(m).start()
-
-    nn, nf = len(near), len(far)
-    for q in range(nn):
+    def grad_rest(m):
+        @pl.loop(0, hid // tn)
+        def _(k):
+            rows, outs, v = grad_tile(1, most, half - most, m, k)
+            p = jnp.maximum(pre[rows, outs].astype(F32), 0.0)
+            gp[rows, outs] = ((grad[rows, outs] + v) * 2.0 * p).astype(BF16)
+
+        gp_copy(m).start()
+
+    def near_in(q):
         near_copies[q].wait_recv()
-        product(q)
-    grad_first()
-
-    done2 = 0
-    done3 = 0
-    for q in range(nf):
-        while done2 < min(nn + q - 1, (q * (nn + nf)) // nf):
-            second(done2)
-            done2 += 1
+
+    def far_in(q):
         x_copies[q].wait_recv()
         fwd_copy(q).start()
+
+    def far_both(q):
         fwd_copy(q).wait_recv()
-        product(nn + q)
-    grad_rest()
+
+    nn, nf = len(near), len(far)
     total = nn + nf
-    while done2 < total:
-        second(done2)
-        done2 += 1
-        while done3 < done2 - 2:
-            last(done3)
-            done3 += 1
-    while done3 < total:
-        last(done3)
-        done3 += 1
+    steps = {
+        "A": lambda j: product(j, False), "B": lambda j: product(j, True),
+        "s": second, "t": third, "l": last, "n": near_in, "x": far_in, "f": far_both,
+        "g": grad_first, "h": grad_next, "e": grad_rest, "o": turn_own, "i": turn_in,
+    }
+    loads[0].wait()
+    turn_own(0)
+    loads[1].wait()
+    loads[2].wait()
+    turn_in(0)
+    for step in " ".join(order).split():
+        steps[step[0]](int(step[1:]))
     out = local(3, gw, gw_hbm)
     out.start()
 
@@ -269,11 +337,9 @@
         fwd_copy(q).wait_send()
     for j in range(total):
         y_copy(j).wait_send()
-        for d in range(1, depth):
-            z_copy(j, d).wait_send()
-
-    @pl.loop(0, tokens // tm)
-    def _(m):
+        for kind in ("up", "down", "two"):
+            z_copy(j, kind).wait_send()
+    for m in range(tokens // tm):
         gp_copy(m).wait()
     out.wait()
 
@@ -287,8 +353,8 @@
         half = cotangent.shape[1]
         width = down_weight.shape[1]
         block = hid // reps
-        if not (fs == 2 and tp == 1 and depth * CORES * ROWS == reps and depth % 2 == 0
-                and block % 128 == 0 and half % 1024 == 0 and hid % 512 == 0 and tokens % 256 == 0):
+        if not (fs == 2 and tp == 1 and depth * CORES * ROWS == reps and depth == 4
+                and block % 128 == 0 and half % 1024 == 0 and hid % 512 == 0 and tokens == 1024):
             return plain(pre_act, down_weight, cotangent)
         step = half // 4
         near = chunks_of(half, [step] * 4)
@@ -299,7 +365,7 @@
         dma = lambda n: pltpu.SemaphoreType.DMA((n,))
         vm = pltpu.VMEM
         return pl.pallas_call(
-            functools.partial(kernel, depth, near, far, factor),
+            functools.partial(kernel, depth, near, far, step * 2, ORDER, factor),
             out_shape=[
                 jax.ShapeDtypeStruct((tokens, hid), BF16),
                 jax.ShapeDtypeStruct((block, width), F32),
@@ -318,10 +384,10 @@
                 vm((depth, block, width), BF16),
                 vm((depth, block, width), F32),
                 vm((depth, block, width), BF16),
-                vm((depth - 1, block, width), BF16),
+                vm((depth, block, width), BF16),
                 vm((block, width), F32),
                 dma(4), dma(2 * depth), dma(2 * depth), dma(nn), dma(nn), dma(nf), dma(nf), dma(nf), dma(nf),
-                dma(total), dma(total), dma(total * (depth - 1)), dma(total * (depth - 1)),
+                dma(total), dma(total), dma(total * depth), dma(total * depth),
                 dma(tokens // 256),
             ],
             compiler_params=pltpu.CompilerParams(

time: 86 us -> 75.8 us (0.88)
  Pallas kernels: 79.4 us -> 69.1 us
    pallas_call x1, Pallas kernels: 79.4 us -> 69.1 us  [on_device(): pl.pallas_call(functools.partial(kernel, depth, near, far, step * 2, ORDE...]
where the time goes in v2:
time: 75.8 us; the launch traced here: 75.6 us
  Pallas kernels  69.1 us (91%)
  local copies, waits for them, and re-layouts  5.85 us (8%)
    pallas_call x1, Pallas kernels, on_device(): pl.pallas_call(functools.partial(kernel, depth, near, far, step * 2, ORDE...  69.1 us
    unnamed x4, local copies, waits for them, and re-layouts  5.85 us

profile of v2, /device:TPU:0, one launch (start us, length us, event | category | flops | bytes accessed | tf_op | source)
XLA Modules:
  0.0 75.6 jit_solution(12157952010911760170)
XLA Ops:
  0.6 69.1 %shard_map.50 = (bf16[1024,2048]{1,0:T(8,128)(2,1)}, f32[128,2048]{1,0:T(8,128)}) custom-call(bf16[1024,2048]{1,0:T(8,128)(2,1)} %pre_hbm.1, bf16[2048,2048]{1,0:T(8,128)(2,1)} %w_hbm.1, bf16[1024,1024]{1,0:T(8,128)(2,1)} %cot_hbm.1), custom_call_target="tpu_custom_call" | custom-call | flops 17179869184 | bytes 41943040 | tf_op jit(solution)/shard_map/pallas_call | solution.py:367
  69.8 0.0 copy-start
  69.8 4.9 %copy.7 = bf16[1024,2048]{1,0:T(8,128)(2,1)} copy(bf16[1024,2048]{1,0:T(8,128)(2,1)} %get-tuple-element.4) | data formatting | bytes 8388608
  74.6 0.0 copy-done
  74.6 1.0 %copy.8 = f32[128,2048]{1,0:T(8,128)} copy(f32[128,2048]{1,0:T(8,128)S(1)} %copy-done) | data formatting | bytes 2097152
Async XLA Ops:
  69.8 4.9 %copy-start = (f32[128,2048]{1,0:T(8,128)S(1)}, f32[128,2048]{1,0:T(8,128)}, u32[]{:S(2)}) copy-start(f32[128,2048]{1,0:T(8,128)} %get-tuple-element.5) | copy-start | bytes 3145732

commit v3 on v2

--- a/solution.py
+++ b/solution.py
@@ -18,19 +18,19 @@
     "n2 A2 n3 A3",
     "s0 B2 x0 B3",
     "f0 A4 B4 s1",
-    "g0 g1 x1 t0",
-    "g2 f1 s2 A5",
-    "B5 t1 g3 h0",
-    "t2 h1 s3 h2",
-    "h3 l0 t3 s4",
-    "x2 l1 f2 A6",
-    "B6 s5 t4 l2",
-    "x3 l3 f3 A7",
-    "B7 s6 x4 t5",
-    "f4 A8 B8 s7",
-    "e0 t6 l4 e1",
-    "s8 e2 l5 l6",
-    "e3 l7 l8",
+    "g0 g1 t0 g2",
+    "x1 s2 f1 A5",
+    "B5 g3 t1 h0",
+    "h1 s3 h2 t2",
+    "h3 x2 s4 l0",
+    "f2 A6 B6 t3",
+    "s5 l1 x3 t4",
+    "f3 A7 B7 t5",
+    "l2 x4 s6 f4",
+    "A8 B8 s7 e0",
+    "t6 l3 e1 s8",
+    "l4 e2 l5 e3",
+    "l6 l7 l8",
 )
 
 
@@ -61,11 +61,11 @@
 
 def kernel(
     depth, near, far, most, order, factor,
-    pre_hbm, w_hbm, cot_hbm, gp_hbm, gw_hbm,
-    pre, pre_in, turned, w, cot, grad, gp,
-    y_out, y_in, own, z_out, z_in, gw,
+    pre_hbm, w_hbm, cot_hbm, gp, gw,
+    pre, pre_in, turned, w, cot, grad,
+    y_out, y_in, own, z_out, z_in,
     s_local, s_pre_s, s_pre_r, s_near_s, s_near_r, s_x_s, s_x_r, s_fwd_s, s_fwd_r,
-    s_y_s, s_y_r, s_z_s, s_z_r, s_gp,
+    s_y_s, s_y_r, s_z_s, s_z_r,
 ):
     rep, fs, tp = lax.axis_index("rep"), lax.axis_index("fs"), lax.axis_index("tp")
     c, y, z = rep % CORES, (rep // CORES) % ROWS, rep // (CORES * ROWS)
@@ -114,13 +114,14 @@
     for i in range(blocks):
         pre_copies.append(remote(
             pre_hbm.at[:, columns(i, 1 - c)], pre_in.at[i], s_pre_s.at[i], s_pre_r.at[i], partner))
-        pre_copies[-1].start()
     near_copies = []
     for q, (a, n) in enumerate(near):
         near_copies.append(remote(
             cot_hbm.at[:, pl.ds(a, n)], cot.at[0, pl.ds(tokens, tokens), pl.ds(a, n)],
             s_near_s.at[q], s_near_r.at[q], partner))
-        near_copies[-1].start()
+    for group in (pre_copies[:depth], near_copies[:2], pre_copies[depth:], near_copies[2:]):
+        for copy in group:
+            copy.start()
     for xc in x_copies[1:]:
         xc.start()
 
@@ -280,6 +281,9 @@
             preferred_element_type=F32)
 
     def grad_first(m):
+        if m == 0:
+            loads[2].wait()
+
         @pl.loop(0, hid // tn)
         def _(k):
             rows, outs, v = grad_tile(0, 0, half, m, k)
@@ -290,10 +294,6 @@
         def _(k):
             rows, outs, v = grad_tile(1, 0, most, m, k)
             grad[rows, outs] += v
-
-    def gp_copy(m):
-        rows = pl.ds(m * tm, tm)
-        return pltpu.make_async_copy(gp.at[rows], gp_hbm.at[rows], s_gp.at[m])
 
     def grad_rest(m):
         @pl.loop(0, hid // tn)
@@ -301,8 +301,6 @@
             rows, outs, v = grad_tile(1, most, half - most, m, k)
             p = jnp.maximum(pre[rows, outs].astype(F32), 0.0)
             gp[rows, outs] = ((grad[rows, outs] + v) * 2.0 * p).astype(BF16)
-
-        gp_copy(m).start()
 
     def near_in(q):
         near_copies[q].wait_recv()
@@ -324,12 +322,9 @@
     loads[0].wait()
     turn_own(0)
     loads[1].wait()
-    loads[2].wait()
     turn_in(0)
     for step in " ".join(order).split():
         steps[step[0]](int(step[1:]))
-    out = local(3, gw, gw_hbm)
-    out.start()
 
     for copy in pre_copies + near_copies + x_copies:
         copy.wait_send()
@@ -339,9 +334,6 @@
         y_copy(j).wait_send()
         for kind in ("up", "down", "two"):
             z_copy(j, kind).wait_send()
-    for m in range(tokens // tm):
-        gp_copy(m).wait()
-    out.wait()
 
 
 def solution(mesh):
@@ -367,11 +359,11 @@
         return pl.pallas_call(
             functools.partial(kernel, depth, near, far, step * 2, ORDER, factor),
             out_shape=[
-                jax.ShapeDtypeStruct((tokens, hid), BF16),
-                jax.ShapeDtypeStruct((block, width), F32),
+                pltpu.VMEM((tokens, hid), BF16),
+                pltpu.VMEM((block, width), F32),
             ],
             in_specs=[pl.BlockSpec(memory_space=pl.ANY)] * 3,
-            out_specs=[pl.BlockSpec(memory_space=pl.ANY)] * 2,
+            out_specs=[pl.BlockSpec(memory_space=pltpu.VMEM)] * 2,
             scratch_shapes=[
                 vm((tokens, hid), BF16),
                 vm((2 * depth, tokens, block), BF16),
@@ -379,19 +371,16 @@
                 vm(down_weight.shape, BF16),
                 vm((2, 2 * tokens, half), BF16),
                 vm((tokens, hid), F32),
-                vm((tokens, hid), BF16),
                 vm((depth, block, width), BF16),
                 vm((depth, block, width), BF16),
                 vm((depth, block, width), F32),
                 vm((depth, block, width), BF16),
                 vm((depth, block, width), BF16),
-                vm((block, width), F32),
                 dma(4), dma(2 * depth), dma(2 * depth), dma(nn), dma(nn), dma(nf), dma(nf), dma(nf), dma(nf),
                 dma(total), dma(total), dma(total * depth), dma(total * depth),
-                dma(tokens // 256),
             ],
             compiler_params=pltpu.CompilerParams(
-                collective_id=0, has_side_effects=True, vmem_limit_bytes=66 * 1000 * 1000
+                collective_id=0, has_side_effects=True, vmem_limit_bytes=54 * 1024 * 1024
             ),
             cost_estimate=pl.CostEstimate(
                 flops=8 * tokens * hid * width // 2, bytes_accessed=40 * 1024 * 1024, transcendentals=0),

time: 75.8 us -> 70.7 us (0.933)
  local copies, waits for them, and re-layouts: 5.85 us -> 2.99 us
  Pallas kernels: 69.1 us -> 66.9 us
    unnamed x4 -> x2, local copies, waits for them, and re-layouts: 5.85 us -> 2.99 us
    pallas_call x1, Pallas kernels: 69.1 us -> 66.9 us  [on_device(): pl.pallas_call(functools.partial(kernel, depth, near, far, step * 2, ORDE...]
where the time goes in v3:
time: 70.7 us; the launch traced here: 70.5 us
  Pallas kernels  66.9 us (95%)
  local copies, waits for them, and re-layouts  2.99 us (4%)
    pallas_call x1, Pallas kernels, on_device(): pl.pallas_call(functools.partial(kernel, depth, near, far, step * 2, ORDE...  66.9 us
    unnamed x2, local copies, waits for them, and re-layouts  2.99 us

profile of v3, /device:TPU:0, one launch (start us, length us, event | category | flops | bytes accessed | tf_op | source)
XLA Modules:
  0.0 70.5 jit_solution(5555221362061521947)
XLA Ops:
  0.6 66.9 %shard_map.50 = (bf16[1024,2048]{1,0:T(8,128)(2,1)S(1)}, f32[128,2048]{1,0:T(8,128)S(1)}) custom-call(bf16[1024,2048]{1,0:T(8,128)(2,1)} %pre_hbm.1, bf16[2048,2048]{1,0:T(8,128)(2,1)} %w_hbm.1, bf16[1024,1024]{1,0:T(8,128)(2,1)} %cot_hbm.1), custom_call_target="tpu_custom_call" | custom-call | flops 17179869184 | bytes 41943040 | tf_op jit(solution)/shard_map/pallas_call | solution.py:359
  67.5 2.0 %copy.7 = bf16[1024,2048]{1,0:T(8,128)(2,1)} copy(bf16[1024,2048]{1,0:T(8,128)(2,1)S(1)} %get-tuple-element.2) | data formatting | bytes 8388608
  69.6 1.0 %copy.8 = f32[128,2048]{1,0:T(8,128)} copy(f32[128,2048]{1,0:T(8,128)S(1)} %get-tuple-element.3) | data formatting | bytes 2097152
